TPU v7x, 32 devices: a whole 2x2x4 slice. The times are simulated.
32 devices in a mesh: grp: 2 (over y), sp: 4 (over z), tp: 4 (over x, core).
Axes of the slice: x: 2, y: 2, z: 4, core: 2. Of those that a mesh axis runs over, the one named last changes fastest.
Arguments:
- residual: bfloat16 [2048, 2048], P(('grp', 'sp')), parts along dimension 0, may hold values from -6 to 6
- queries: bfloat16 [2048, 1024], P(('grp', 'sp'), 'tp'), parts along dimension 0, may hold values from -400 to 400
- keys: bfloat16 [2048, 1024], P(('grp', 'sp'), 'tp'), parts along dimension 0, may hold values from -8 to 8
- values: bfloat16 [2048, 1024], P(('grp', 'sp'), 'tp'), parts along dimension 0, may hold values from -6 to 6
- log_gates: float32 [2048, 16], P(('grp', 'sp'), 'tp'), parts along dimension 0, may hold values from -126 to 0, as said below
- w_out: bfloat16 [1024, 2048], P('tp'), may hold values from -0.75 to 0.75
- norm_gain: float32 [2048], replicated, may hold values from 0.1 to 1.9
- w_gate: bfloat16 [2048, 5632], P('sp', 'tp'), may hold values from -0.125 to 0.125
- w_up: bfloat16 [2048, 5632], P('sp', 'tp'), may hold values from -0.125 to 0.125
- w_down: bfloat16 [5632, 2048], P('tp', 'sp'), may hold values from -0.078125 to 0.078125
Outputs:
- output: bfloat16 [2048, 2048], P(('grp', 'sp', 'tp')), parts along dimension 0
There are 2 independent parts, one for each index of `grp`. A program takes and returns all parts, laid end to end along the dimension named above; an argument that names none is the same for every part. Nothing has to cross between parts.
Inputs may be any that keep to these rules, and one draw needn't show every extreme that they name: `log_gates`: never rises along positions.
All inputs are finite; a program needn't handle non-finite values.
Results may differ from a plain program's by a relative error of at most 0.014.
Values may be sent and summed in bfloat16 or wider, within the bound.
A program may use at most 128 MiB of HBM per device.

v0:
```python
import math
import jax
import jax.numpy as jnp
from jax import lax
from jax.sharding import PartitionSpec as P


def normalize(rows_in, gain):
    floats = rows_in.astype(jnp.float32)
    scaled = floats * lax.rsqrt(jnp.mean(floats * floats, axis=-1, keepdims=True) + 1e-06)
    return (scaled * gain).astype(jnp.bfloat16)


def attend(queries, keys, values, log_gates):
    row_count = queries.shape[0]
    head_count = log_gates.shape[1]
    head_width = queries.shape[1] // head_count
    score_scale = head_width ** (-0.5)
    first_row = lax.axis_index("sp") * row_count
    query_heads = queries.reshape(row_count, head_count, head_width)
    query_gates = log_gates.T
    query_positions = first_row + jnp.arange(row_count, dtype=jnp.int32)
    initial = (
        jnp.full((head_count, row_count), -1e30, jnp.float32),
        jnp.zeros((head_count, row_count), jnp.float32),
        jnp.zeros((head_count, row_count, head_width), jnp.float32),
    )
    carried = initial
    key_piece = lax.all_gather(keys.astype(jnp.float32), "sp", axis=0, tiled=True).astype(
        jnp.bfloat16
    )
    value_piece = lax.all_gather(values.astype(jnp.float32), "sp", axis=0, tiled=True).astype(
        jnp.bfloat16
    )
    gate_piece = lax.all_gather(log_gates, "sp", axis=0, tiled=True)
    length = key_piece.shape[0]
    block_rows = math.gcd(length, 2048)
    block_count = length // block_rows
    key_blocks = key_piece.reshape(block_count, block_rows, head_count, head_width)
    value_blocks = value_piece.reshape(block_count, block_rows, head_count, head_width)
    gate_blocks = gate_piece.reshape(block_count, block_rows, head_count)
    offsets = jnp.arange(block_count, dtype=jnp.int32) * block_rows

    def one_block(state, inputs):
        current_key_block, value_block, gate_block, offset = inputs

        def work(current):
            running_max, running_sum, accumulated = current
            scores = (
                jnp.einsum(
                    "qhd,khd->hqk",
                    query_heads,
                    current_key_block,
                    preferred_element_type=jnp.float32,
                )
                * score_scale
            )
            scores = scores + query_gates[:, :, None] - gate_block.T[:, None, :]
            key_positions = offset + jnp.arange(block_rows, dtype=jnp.int32)
            causal = (query_positions[:, None] >= key_positions[None, :])[None]
            scores = jnp.where(causal, scores, -1e30)
            new_max = jnp.maximum(running_max, jnp.max(scores, axis=-1))
            weights = jnp.where(causal, jnp.exp(scores - new_max[:, :, None]), 0.0)
            rescale = jnp.exp(running_max - new_max)
            running_sum = running_sum * rescale + jnp.sum(weights, axis=-1)
            product = jnp.einsum(
                "hqk,khd->hqd",
                weights.astype(jnp.bfloat16),
                value_block,
                preferred_element_type=jnp.float32,
            )
            accumulated = accumulated * rescale[:, :, None] + product
            return (new_max, running_sum, accumulated)

        state = lax.cond(offset <= first_row + row_count - 1, work, lambda current: current, state)
        return (state, None)

    carried, _ = lax.scan(one_block, carried, (key_blocks, value_blocks, gate_blocks, offsets))
    running_max, running_sum, accumulated = carried
    attended = accumulated / running_sum[:, :, None]
    return (
        attended.transpose(1, 0, 2).reshape(row_count, head_count * head_width).astype(jnp.bfloat16)
    )


def body(residual, queries, keys, values, log_gates, w_out, norm_gain, w_gate, w_up, w_down):
    attended = attend(queries, keys, values, log_gates)
    row_count = attended.shape[0]
    per_device = row_count // lax.axis_size("tp")
    my_first = lax.axis_index("tp") * per_device
    projected = lax.psum(
        jnp.dot(attended, w_out, preferred_element_type=jnp.float32).astype(jnp.bfloat16), "tp"
    ).astype(jnp.float32)
    mixed_all = (residual.astype(jnp.float32) + projected).astype(jnp.bfloat16)
    normed_all = normalize(mixed_all, norm_gain)
    mixed = lax.dynamic_slice_in_dim(mixed_all, my_first, per_device, 0)
    gate_whole = lax.all_gather(w_gate, "sp", axis=0, tiled=True)
    up_whole = lax.all_gather(w_up, "sp", axis=0, tiled=True)
    down_whole = lax.all_gather(w_down, "sp", axis=1, tiled=True)
    gate_proj = jnp.dot(normed_all, gate_whole, preferred_element_type=jnp.float32)
    up_proj = jnp.dot(normed_all, up_whole, preferred_element_type=jnp.float32)
    hidden = (jax.nn.silu(gate_proj) * up_proj).astype(jnp.bfloat16)
    down_sum = lax.psum_scatter(
        jnp.dot(hidden, down_whole, preferred_element_type=jnp.float32).astype(jnp.bfloat16),
        "tp",
        scatter_dimension=0,
        tiled=True,
    ).astype(jnp.float32)
    summed = mixed.astype(jnp.float32) + 0.5 * down_sum
    scaled = summed * lax.rsqrt(jnp.mean(summed * summed, axis=-1, keepdims=True) + 1e-06)
    return scaled.astype(jnp.bfloat16)


def solution(mesh):
    in_specs = (
        P(("grp", "sp"), None),
        P(("grp", "sp"), "tp"),
        P(("grp", "sp"), "tp"),
        P(("grp", "sp"), "tp"),
        P(("grp", "sp"), "tp"),
        P("tp", None),
        P(),
        P("sp", "tp"),
        P("sp", "tp"),
        P("tp", "sp"),
    )
    out_specs = P(("grp", "sp", "tp"), None)
    return jax.shard_map(body, mesh=mesh, in_specs=in_specs, out_specs=out_specs, check_vma=False)
```

profile of v0, /device:TPU:0, one launch (start us, length us, event | category | flops | bytes accessed | tf_op | source)
XLA Modules:
  0.0 429.7 jit_solution(2206887288210929115)
XLA Ops:
  7.4 1.1 copy.12
  8.5 17.4 %all_gather.18 = bf16[1024,256]{0,1:T(8,128)(2,1)S(1)} all-gather(bf16[256,256]{0,1:T(8,128)(2,1)S(1)} %copy.12), channel_id=1, replica_groups=mesh['grp'=2,'sp'=4,'tp'=4] {'sp'}, dimensions={0}, use_global_device_ids=true | all-gather | bytes 655360 | tf_op jit(solution)/shard_map/all_gather | solution.py:29
  25.8 1.0 copy.13
  26.9 16.3 %all_gather.20 = bf16[1024,256]{0,1:T(8,128)(2,1)S(1)} all-gather(bf16[256,256]{0,1:T(8,128)(2,1)S(1)} %copy.13), channel_id=1, replica_groups=mesh['grp'=2,'sp'=4,'tp'=4] {'sp'}, dimensions={0}, use_global_device_ids=true | all-gather | bytes 655360 | tf_op jit(solution)/shard_map/all_gather | solution.py:32
  43.1 13.3 %all_gather.19 = f32[1024,4]{0,1:T(4,128)S(1)} all-gather(f32[256,4]{0,1:T(4,128)} %param.16), channel_id=1, replica_groups=mesh['grp'=2,'sp'=4,'tp'=4] {'sp'}, dimensions={0}, use_global_device_ids=true | all-gather | bytes 20480 | tf_op jit(solution)/shard_map/all_gather | solution.py:35
  56.5 7.0 %conditional.1 = ((f32[4,256]{1,0:T(4,128)S(1)}, f32[4,256,64]{1,2,0:T(8,128)S(1)})) conditional(s32[]{:T(128)} %convert_element_type.64, (f32[4,256]{1,0:T(4,128)S(1)}, f32[4,256,64]{1,2,0:T(8,128)S(1)}) %tuple.22, (s32[]{:T(128)}, s32[256]{0:T(256)S(1)}, bf16[256,256]{1,0:T(8,128)(2,1)}, bf16[1024,256]{0,1:T(8,128)(2,1)S(1)}, f32[4,256]{1,0:T(4,128)}, ...), branch_computations={%region_0.1_spmd, %region_1.0_spmd} | conditional | flops 288754944 | bytes 15727672 | solution.py:75
  56.8 1.0 copy.14
  57.8 2.1 fusion.2
  59.9 2.0 fusion.1
  61.9 1.6 fusion.6
  63.6 1.4 convolution_convert_fusion
  65.1 0.5 all-gather.4.cloned.1.call-update
  65.7 0.5 all-gather.6.cloned.1.call-update
  66.3 0.5 all-gather.8.cloned.1.call-update
  66.8 35.4 %all-reduce.2.cloned.1.call-done = bf16[256,2048]{1,0:T(8,128)(2,1)} async-done(((bf16[256,2048]{1,0:T(8,128)(2,1)}), bf16[256,2048]{1,0:T(8,128)(2,1)}) %all-reduce.2.cloned.1.call-update) | async-done | bytes 1048592 | tf_op jit(solution)/shard_map/psum | solution.py:91
  102.2 1.7 fusion.13
  104.0 70.1 %all-gather.4.cloned.1.call-done = bf16[2048,1408]{1,0:T(8,128)(2,1)} async-done(((bf16[512,1408]{1,0:T(8,128)(2,1)}), bf16[2048,1408]{1,0:T(8,128)(2,1)}) %all-gather.4.cloned.1.call-update) | async-done | bytes 5767184 | tf_op jit(solution)/shard_map/all_gather | solution.py:97
  174.1 5.6 %fusion.18 = f32[256,1408]{1,0:T(8,128)} fusion(bf16[2048,1408]{1,0:T(8,128)(2,1)} %all-gather.4.cloned.1.call-done, bf16[256,2048]{1,0:T(8,128)(2,1)S(1)} %get-tuple-element.132, f32[2048]{0:T(1024)S(1)} %copy-done.3, f32[256]{0:T(256)S(1)} %add_rsqrt_fusion), kind=kOutput, calls=%fused_computation.29 | convolution fusion | flops 1478492160 | bytes 8266752 | tf_op jit(solution)/shard_map/dot_general | solution.py:100
  179.8 100.6 %all-gather.6.cloned.1.call-done = bf16[2048,1408]{1,0:T(8,128)(2,1)} async-done(((bf16[512,1408]{1,0:T(8,128)(2,1)}), bf16[2048,1408]{1,0:T(8,128)(2,1)}) %all-gather.6.cloned.1.call-update) | async-done | bytes 5767184 | tf_op jit(solution)/shard_map/all_gather | solution.py:98
  280.4 106.3 %all-gather.8.cloned.1.call-done = bf16[1408,2048]{1,0:T(8,128)(2,1)} async-done(((bf16[1408,512]{1,0:T(8,128)(2,1)}), bf16[1408,2048]{1,0:T(8,128)(2,1)}) %all-gather.8.cloned.1.call-update) | async-done | bytes 5767184 | tf_op jit(solution)/shard_map/all_gather | solution.py:99
  386.7 9.3 %convolution_convert_fusion.1 = bf16[256,2048]{1,0:T(8,128)(2,1)} fusion(bf16[1408,2048]{1,0:T(8,128)(2,1)} %all-gather.8.cloned.1.call-done, bf16[2048,1408]{1,0:T(8,128)(2,1)} %all-gather.6.cloned.1.call-done, f32[256,1408]{1,0:T(8,128)} %fusion.18, bf16[256,2048]{1,0:T(8,128)(2,1)S(1)} %get-tuple-element.132, f32[2048]{0:T(1024)S(1)} %copy-done.3, ...), kind=kOutput, calls=%fused_computation.21 | convolution fusion | flops 2957574144 | bytes 15082496 | tf_op jit(solution)/shard_map/dot_general | solution.py:104
  396.0 23.2 %reduce-scatter.2.cloned.1.call-done = bf16[64,2048]{1,0:T(8,128)(2,1)} async-done(((bf16[256,2048]{1,0:T(8,128)(2,1)}), bf16[64,2048]{1,0:T(8,128)(2,1)}) %reduce-scatter.2.cloned.1.call-update) | async-done | bytes 262160 | tf_op jit(solution)/shard_map/reduce_scatter | solution.py:103
  419.2 1.2 multiply_reduce_fusion
  420.4 1.8 multiply_convert_fusion
  (25 shorter events, 0.5 us)
Async XLA Ops:
  7.4 56.2 %copy-start = (bf16[256,2048]{1,0:T(8,128)(2,1)S(1)}, bf16[256,2048]{1,0:T(8,128)(2,1)}, u32[]{:S(2)}) copy-start(bf16[256,2048]{1,0:T(8,128)(2,1)} %param.17) | copy-start | bytes 3145732
  7.4 94.9 %all-reduce.2.cloned.1.call-start = ((), (), s32[]{:S(2)}) async-start(), calls=%async_computation.1 | async-start | bytes 2097152 | tf_op jit(solution)/shard_map/psum | solution.py:91
  56.5 3.3 copy-start.2
  63.5 38.7 %copy-start.1 = (bf16[256,2048]{1,0:T(8,128)(2,1)S(1)}, bf16[256,2048]{1,0:T(8,128)(2,1)}, u32[]{:S(2)}) copy-start(bf16[256,2048]{1,0:T(8,128)(2,1)} %param.12) | copy-start | bytes 3145732
  65.0 109.1 %copy-start.3 = (f32[2048]{0:T(1024)S(1)}, f32[2048]{0:T(1024)}, u32[]{:S(2)}) copy-start(f32[2048]{0:T(1024)} %param.18) | copy-start | bytes 24580
  65.0 109.1 %all-gather.4.cloned.1.call-start = ((), (), s32[]{:S(2)}) async-start(), calls=%async_computation.2 | async-start | bytes 7208960 | tf_op jit(solution)/shard_map/all_gather | solution.py:97
  65.6 214.8 %all-gather.6.cloned.1.call-start = ((), (), s32[]{:S(2)}) async-start(), calls=%async_computation.3 | async-start | bytes 7208960 | tf_op jit(solution)/shard_map/all_gather | solution.py:98
  66.2 320.5 %all-gather.8.cloned.1.call-start = ((), (), s32[]{:S(2)}) async-start(), calls=%async_computation.4 | async-start | bytes 7208960 | tf_op jit(solution)/shard_map/all_gather | solution.py:99
  66.8 352.4 %reduce-scatter.2.cloned.1.call-start = ((), (), s32[]{:S(2)}) async-start(), calls=%async_computation.5 | async-start | bytes 1310720 | tf_op jit(solution)/shard_map/reduce_scatter | solution.py:103
Sparse Core Ops, SparseCore 0:
  65.2 37.0 all-reduce.1
  396.1 23.0 reduce-scatter.1
Sparse Core Ops, SparseCore 1:
  67.1 107.0 all-gather.3
  175.6 104.8 all-gather.5
  281.9 104.8 all-gather.7
where the time goes:
time: 430 us
  waiting for transfers between devices  337 us (78%)
  blocking collectives  47 us (11%)
  matrix products  20 us (5%)
  between operations  15.1 us (4%)
  other arithmetic  6.94 us (2%)
    all_gather x1, waiting for transfers between devices, body(): down_whole = lax.all_gather(w_down, 'sp', axis=1, tiled=True)  106 us
    all_gather x1, waiting for transfers between devices, body(): up_whole = lax.all_gather(w_up, 'sp', axis=0, tiled=True)  101 us
    all_gather x1, waiting for transfers between devices, body(): gate_whole = lax.all_gather(w_gate, 'sp', axis=0, tiled=True)  70.1 us
    psum x1, waiting for transfers between devices, body(): lax.psum(jnp.dot(attended, w_out, preferred_element_type=jnp.float32).ast...  35.4 us
    reduce_scatter x1, waiting for transfers between devices, body(): lax.psum_scatter(jnp.dot(hidden, down_whole, preferred_element_type=jnp.f...  23.2 us
    all_gather x1, blocking collectives, attend(): lax.all_gather(keys.astype(jnp.float32), 'sp', axis=0, tiled=True)  17.4 us
    all_gather x1, blocking collectives, attend(): lax.all_gather(values.astype(jnp.float32), 'sp', axis=0, tiled=True)  16.3 us
    all_gather x1, blocking collectives, attend(): gate_piece = lax.all_gather(log_gates, 'sp', axis=0, tiled=True)  13.3 us
  transfers between devices with their start and end apart: 5, of which 5 were waited for; matrix products, arithmetic and copies ran while one was open for 2% of the time, Pallas kernels for 0%

commit v1 on v0

--- a/solution.py
+++ b/solution.py
@@ -95,7 +95,12 @@
     normed_all = normalize(mixed_all, norm_gain)
     mixed = lax.dynamic_slice_in_dim(mixed_all, my_first, per_device, 0)
     gate_whole = lax.all_gather(w_gate, "sp", axis=0, tiled=True)
-    up_whole = lax.all_gather(w_up, "sp", axis=0, tiled=True)
+    ring = [w_up]
+    for hop in range(3):
+        ring.append(lax.ppermute(ring[-1], "sp", [(dev, (dev + 1) % 4) for dev in range(4)]))
+    up_whole = jnp.roll(
+        jnp.concatenate(ring[::-1], axis=0), (lax.axis_index("sp") + 1) * ring[0].shape[0], axis=0
+    )
     down_whole = lax.all_gather(w_down, "sp", axis=1, tiled=True)
     gate_proj = jnp.dot(normed_all, gate_whole, preferred_element_type=jnp.float32)
     up_proj = jnp.dot(normed_all, up_whole, preferred_element_type=jnp.float32)

time: 430 us -> 386 us (0.90)
  waiting for transfers between devices: 337 us -> 251 us
  starting transfers between devices: 0.17 us -> 27.3 us
  local copies, waits for them, and re-layouts: 3.14 us -> 19.6 us
    ppermute x0 -> x3, waiting for transfers between devices: none -> 151 us  [body(): lax.ppermute(ring[-1], 'sp', [(dev, (dev + 1) % 4) for dev in range(4)])]
    all_gather x1 -> x0, waiting for transfers between devices: 101 us -> none  [body(): up_whole = lax.all_gather(w_up, 'sp', axis=0, tiled=True)]
    all_gather x1, waiting for transfers between devices: 70.1 us -> 0.01 us  [body(): gate_whole = lax.all_gather(w_gate, 'sp', axis=0, tiled=True)]
    psum x1, waiting for transfers between devices: 35.4 us -> 0.01 us  [body(): lax.psum(jnp.dot(attended, w_out, preferred_element_type=jnp.float32).ast...]
    all_gather x1, waiting for transfers between devices: 106 us -> 75 us  [body(): down_whole = lax.all_gather(w_down, 'sp', axis=1, tiled=True)]
    ppermute x0 -> x3, starting transfers between devices: none -> 27.2 us  [body(): lax.ppermute(ring[-1], 'sp', [(dev, (dev + 1) % 4) for dev in range(4)])]
    unnamed x8 -> x19, local copies, waits for them, and re-layouts: 2.1 us -> 17.4 us
  transfers between devices with their start and end apart: 5 -> 7, of which waited for: 5 -> 5; matrix products, arithmetic and copies ran while one was open for 2% -> 6% of each run, Pallas kernels for 0% -> 0%
where the time goes in v1:
time: 386 us; the launch traced here: 385 us
  waiting for transfers between devices  251 us (65%)
  blocking collectives  47 us (12%)
  starting transfers between devices  27.3 us (7%)
  local copies, waits for them, and re-layouts  19.6 us (5%)
  matrix products  18.5 us (5%)
  between operations  15 us (4%)
  other arithmetic  7.37 us (2%)
    ppermute x3, waiting for transfers between devices, body(): lax.ppermute(ring[-1], 'sp', [(dev, (dev + 1) % 4) for dev in range(4)])  151 us
    all_gather x1, waiting for transfers between devices, body(): down_whole = lax.all_gather(w_down, 'sp', axis=1, tiled=True)  75 us
    ppermute x3, starting transfers between devices, body(): lax.ppermute(ring[-1], 'sp', [(dev, (dev + 1) % 4) for dev in range(4)])  27.2 us
    reduce_scatter x1, waiting for transfers between devices, body(): lax.psum_scatter(jnp.dot(hidden, down_whole, preferred_element_type=jnp.f...  23.2 us
    unnamed x19, local copies, waits for them, and re-layouts  17.4 us
    all_gather x1, blocking collectives, attend(): lax.all_gather(keys.astype(jnp.float32), 'sp', axis=0, tiled=True)  17.4 us
    all_gather x1, blocking collectives, attend(): lax.all_gather(values.astype(jnp.float32), 'sp', axis=0, tiled=True)  16.3 us
    all_gather x1, blocking collectives, attend(): gate_piece = lax.all_gather(log_gates, 'sp', axis=0, tiled=True)  13.3 us
  transfers between devices with their start and end apart: 7, of which 5 were waited for; matrix products, arithmetic and copies ran while one was open for 6% of the time, Pallas kernels for 0%

profile of v1, /device:TPU:0, one launch (start us, length us, event | category | flops | bytes accessed | tf_op | source)
XLA Modules:
  0.0 385.5 jit_solution(1594638843056775709)
XLA Ops:
  8.5 17.4 %all_gather.15 = bf16[1024,256]{0,1:T(8,128)(2,1)S(1)} all-gather(bf16[256,256]{0,1:T(8,128)(2,1)S(1)} %copy.12), channel_id=1, replica_groups=mesh['grp'=2,'sp'=4,'tp'=4] {'sp'}, dimensions={0}, use_global_device_ids=true | all-gather | bytes 655360 | tf_op jit(solution)/shard_map/all_gather | solution.py:29
  26.9 16.3 %all_gather.17 = bf16[1024,256]{0,1:T(8,128)(2,1)S(1)} all-gather(bf16[256,256]{0,1:T(8,128)(2,1)S(1)} %copy.13), channel_id=1, replica_groups=mesh['grp'=2,'sp'=4,'tp'=4] {'sp'}, dimensions={0}, use_global_device_ids=true | all-gather | bytes 655360 | tf_op jit(solution)/shard_map/all_gather | solution.py:32
  43.1 13.3 %all_gather.16 = f32[1024,4]{0,1:T(4,128)S(1)} all-gather(f32[256,4]{0,1:T(4,128)} %param.16), channel_id=1, replica_groups=mesh['grp'=2,'sp'=4,'tp'=4] {'sp'}, dimensions={0}, use_global_device_ids=true | all-gather | bytes 20480 | tf_op jit(solution)/shard_map/all_gather | solution.py:35
  56.5 7.0 %conditional.1 = ((f32[4,256]{1,0:T(4,128)S(1)}, f32[4,256,64]{1,2,0:T(8,128)S(1)})) conditional(s32[]{:T(128)} %convert_element_type.64, (f32[4,256]{1,0:T(4,128)S(1)}, f32[4,256,64]{1,2,0:T(8,128)S(1)}) %tuple.22, (s32[]{:T(128)}, s32[256]{0:T(256)S(1)}, bf16[256,256]{1,0:T(8,128)(2,1)}, bf16[1024,256]{0,1:T(8,128)(2,1)S(1)}, f32[4,256]{1,0:T(4,128)}, ...), branch_computations={%region_0.1_spmd, %region_1.0_spmd} | conditional | flops 288754944 | bytes 15727672 | solution.py:75
  57.8 2.0 fusion.2
  59.9 2.0 fusion.1
  61.9 1.6 fusion.6
  63.6 1.5 convolution_convert_fusion
  67.4 53.2 %collective-permute-done = bf16[512,1408]{1,0:T(8,128)(2,1)S(1)} collective-permute-done((bf16[512,1408]{1,0:T(8,128)(2,1)S(1)}, bf16[512,1408]{1,0:T(8,128)(2,1)S(1)}, u32[]{:S(2)}, u32[]{:S(2)}) %collective-permute-start) | collective-permute-done | bytes 1441824 | tf_op jit(solution)/shard_map/ppermute | solution.py:100
  121.7 13.6 %collective-permute-start.1 = (bf16[512,1408]{1,0:T(8,128)(2,1)S(1)}, bf16[512,1408]{1,0:T(8,128)(2,1)}, u32[]{:S(2)}, u32[]{:S(2)}) collective-permute-start(bf16[512,1408]{1,0:T(8,128)(2,1)S(1)} %collective-permute-done), channel_id=1, source_target_pairs={{0,4},{4,8},{8,12},{12,0},{1,5},{5,9},{9,13},{13,1},{2,6},{6,10},{... | collective-permute-start | bytes 4325384 | tf_op jit(solution)/shard_map/ppermute | solution.py:100
  135.3 67.3 %collective-permute-done.1 = bf16[512,1408]{1,0:T(8,128)(2,1)} collective-permute-done((bf16[512,1408]{1,0:T(8,128)(2,1)S(1)}, bf16[512,1408]{1,0:T(8,128)(2,1)}, u32[]{:S(2)}, u32[]{:S(2)}) %collective-permute-start.1) | collective-permute-done | bytes 1441824 | tf_op jit(solution)/shard_map/ppermute | solution.py:100
  202.6 12.6 %collective-permute-start.2 = (bf16[512,1408]{1,0:T(8,128)(2,1)}, bf16[512,1408]{1,0:T(8,128)(2,1)}, u32[]{:S(2)}, u32[]{:S(2)}) collective-permute-start(bf16[512,1408]{1,0:T(8,128)(2,1)} %collective-permute-done.1), channel_id=1, source_target_pairs={{0,4},{4,8},{8,12},{12,0},{1,5},{5,9},{9,13},{13,1},{2,6},{6,10},{... | collective-permute-start | bytes 4325384 | tf_op jit(solution)/shard_map/ppermute | solution.py:100
  215.2 2.2 fusion.20
  217.3 30.8 %collective-permute-done.2 = bf16[512,1408]{1,0:T(8,128)(2,1)} collective-permute-done((bf16[512,1408]{1,0:T(8,128)(2,1)}, bf16[512,1408]{1,0:T(8,128)(2,1)}, u32[]{:S(2)}, u32[]{:S(2)}) %collective-permute-start.2) | collective-permute-done | bytes 1441824 | tf_op jit(solution)/shard_map/ppermute | solution.py:100
  248.1 2.6 constant_dynamic-update-slice_fusion.7
  250.7 2.6 constant_dynamic-update-slice_fusion.6
  255.8 2.6 constant_dynamic-update-slice_fusion.3
  258.4 2.7 constant_dynamic-update-slice_fusion.2
  261.1 1.3 constant_dynamic-update-slice_fusion.1
  263.5 4.5 %fusion.28 = f32[256,1408]{1,0:T(8,128)S(1)} fusion(bf16[2048,1408]{1,0:T(8,128)(2,1)} %all-gather.3.cloned.1.call-done, bf16[256,2048]{1,0:T(8,128)(2,1)S(1)} %get-tuple-element.132, f32[2048]{0:T(1024)S(1)} %copy-done.5, f32[256]{0:T(256)S(1)} %add_rsqrt_fusion), kind=kOutput, calls=%fused_computation.32 | convolution fusion | flops 1478492160 | bytes 8266752 | tf_op jit(solution)/shard_map/dot_general | solution.py:105
  268.0 75.0 %all-gather.5.cloned.1.call-done = bf16[1408,2048]{1,0:T(8,128)(2,1)} async-done(((bf16[1408,512]{1,0:T(8,128)(2,1)}), bf16[1408,2048]{1,0:T(8,128)(2,1)}) %all-gather.5.cloned.1.call-update) | async-done | bytes 5767184 | tf_op jit(solution)/shard_map/all_gather | solution.py:104
  343.0 8.9 %convolution_convert_fusion.1 = bf16[256,2048]{1,0:T(8,128)(2,1)} fusion(bf16[1408,2048]{1,0:T(8,128)(2,1)} %all-gather.5.cloned.1.call-done, bf16[4096,1408]{1,0:T(8,128)(2,1)} %constant_dynamic-update-slice_fusion, s32[]{:T(128)S(6)} %select_n.29, f32[256,1408]{1,0:T(8,128)S(1)} %fusion.28, bf16[256,2048]{1,0:T(8,128)(2,1)S(1)} %get-tuple-element.132, ...), kind=kOutput, calls=%fused_computation.23 | convolution fusion | flops 2957574144 | bytes 15082500 | tf_op jit(solution)/shard_map/dot_general | solution.py:109
  351.9 23.2 %reduce-scatter.2.cloned.1.call-done = bf16[64,2048]{1,0:T(8,128)(2,1)} async-done(((bf16[256,2048]{1,0:T(8,128)(2,1)}), bf16[64,2048]{1,0:T(8,128)(2,1)}) %reduce-scatter.2.cloned.1.call-update) | async-done | bytes 262160 | tf_op jit(solution)/shard_map/reduce_scatter | solution.py:108
  376.3 1.8 multiply_convert_fusion
  (40 shorter events, 11.6 us)
Async XLA Ops:
  7.4 56.2 %copy-start = (bf16[256,2048]{1,0:T(8,128)(2,1)S(1)}, bf16[256,2048]{1,0:T(8,128)(2,1)}, u32[]{:S(2)}) copy-start(bf16[256,2048]{1,0:T(8,128)(2,1)} %param.17) | copy-start | bytes 3145732
  7.4 207.8 %all-reduce.2.cloned.1.call-start = ((), (), s32[]{:S(2)}) async-start(), calls=%async_computation.1 | async-start | bytes 2097152 | tf_op jit(solution)/shard_map/psum | solution.py:91
  56.5 3.3 copy-start.4
  63.5 2.8 copy-start.1
  65.1 198.5 %all-gather.3.cloned.1.call-start = ((), (), s32[]{:S(2)}) async-start(), calls=%async_computation.2 | async-start | bytes 7208960 | tf_op jit(solution)/shard_map/all_gather | solution.py:97
  65.7 277.4 %all-gather.5.cloned.1.call-start = ((), (), s32[]{:S(2)}) async-start(), calls=%async_computation.3 | async-start | bytes 7208960 | tf_op jit(solution)/shard_map/all_gather | solution.py:104
  66.2 308.9 %reduce-scatter.2.cloned.1.call-start = ((), (), s32[]{:S(2)}) async-start(), calls=%async_computation.4 | async-start | bytes 1310720 | tf_op jit(solution)/shard_map/reduce_scatter | solution.py:108
  66.3 54.3 %collective-permute-start = (bf16[512,1408]{1,0:T(8,128)(2,1)S(1)}, bf16[512,1408]{1,0:T(8,128)(2,1)S(1)}, u32[]{:S(2)}, u32[]{:S(2)}) collective-permute-start(bf16[512,1408]{1,0:T(8,128)(2,1)S(1)} %copy-done.1), channel_id=1, source_target_pairs={{0,4},{4,8},{8,12},{12,0},{1,5},{5,9},{9,13},{13,1},{2,6},{6,10},{... | collective-permute-start | bytes 4325384 | tf_op jit(solution)/shard_map/ppermute | solution.py:100
  120.6 1.1 copy-start.2
  121.7 80.9 %collective-permute-start.1 = (bf16[512,1408]{1,0:T(8,128)(2,1)S(1)}, bf16[512,1408]{1,0:T(8,128)(2,1)}, u32[]{:S(2)}, u32[]{:S(2)}) collective-permute-start(bf16[512,1408]{1,0:T(8,128)(2,1)S(1)} %collective-permute-done), channel_id=1, source_target_pairs={{0,4},{4,8},{8,12},{12,0},{1,5},{5,9},{9,13},{13,1},{2,6},{6,10},{... | collective-permute-start | bytes 4325384 | tf_op jit(solution)/shard_map/ppermute | solution.py:100
  202.6 45.5 %collective-permute-start.2 = (bf16[512,1408]{1,0:T(8,128)(2,1)}, bf16[512,1408]{1,0:T(8,128)(2,1)}, u32[]{:S(2)}, u32[]{:S(2)}) collective-permute-start(bf16[512,1408]{1,0:T(8,128)(2,1)} %collective-permute-done.1), channel_id=1, source_target_pairs={{0,4},{4,8},{8,12},{12,0},{1,5},{5,9},{9,13},{13,1},{2,6},{6,10},{... | collective-permute-start | bytes 4325384 | tf_op jit(solution)/shard_map/ppermute | solution.py:100
  215.2 38.1 %copy-start.3 = (bf16[512,1408]{1,0:T(8,128)(2,1)S(1)}, bf16[512,1408]{1,0:T(8,128)(2,1)}, u32[]{:S(2)}) copy-start(bf16[512,1408]{1,0:T(8,128)(2,1)} %copy-done.2) | copy-start | bytes 4325380
  258.4 5.2 %copy-start.5 = (f32[2048]{0:T(1024)S(1)}, f32[2048]{0:T(1024)}, u32[]{:S(2)}) copy-start(f32[2048]{0:T(1024)} %param.18) | copy-start | bytes 24580
Sparse Core Ops, SparseCore 0:
  65.2 36.9 all-reduce.1
  352.0 23.0 reduce-scatter.1
Sparse Core Ops, SparseCore 1:
  67.1 167.4 all-gather.2
  236.0 106.9 all-gather.4
